TPU v7x, 32 devices: a whole 2x2x4 slice. The times are simulated.
32 devices in a mesh: ep: 8 (over z, y), tp: 4 (over x, core).
Axes of the slice: x: 2, y: 2, z: 4, core: 2. Of those that a mesh axis runs over, the one named last changes fastest.
Arguments:
- queries: bfloat16 [1536, 2048], P('ep', 'tp'), may hold values from -5 to 5
- keys: bfloat16 [1536, 512], P('ep', 'tp'), may hold values from -5 to 5
- values: bfloat16 [1536, 512], P('ep', 'tp'), may hold values from -6 to 6
- query_gain: float32 [128], replicated, may hold values from 0.6 to 6
- key_gain: float32 [128], replicated, may hold values from 0.6 to 6
- out_weight: bfloat16 [2048, 2048], P('tp'), may hold values from -0.125 to 0.125
- mixer_gain: float32 [2048], replicated, may hold values from 0.1 to 1.9
- expert_in: bfloat16 [4096, 2048], P(('ep', 'tp')), may hold values from -6 to 6
- routes: int32 [4096, 2], P(('ep', 'tp')), may hold values from 0 to 7, all different within a row; in each aligned block of 128 rows (0 to 127, 128 to 255, ...) at most 48 rows name the same one
- route_weights: float32 [4096, 2], P(('ep', 'tp')), may hold values from 0.2 to 1
- expert_gain: float32 [2048], replicated, may hold values from 0.5 to 4
- gate_w: bfloat16 [8, 2048, 2048], P('ep', None, 'tp'), may hold values from -0.125 to 0.125
- up_w: bfloat16 [8, 2048, 2048], P('ep', None, 'tp'), may hold values from -0.125 to 0.125
- down_w: bfloat16 [8, 2048, 2048], P('ep', 'tp'), may hold values from -0.125 to 0.125
- ffn_out_gain: float32 [2048], replicated, may hold values from 0.1 to 1.9
Outputs:
- mixer_out: bfloat16 [1536, 2048], P(('ep', 'tp'))
- expert_out: bfloat16 [4096, 2048], P(('ep', 'tp'))
Inputs may be any that keep to these rules, and one draw needn't show every extreme that they name: `routes`: each row names 2 different experts. Among the rows of one device no expert is named by more than 48 rows, and in every draw some expert is named by exactly 48 rows of some device.
All inputs are finite; a program needn't handle non-finite values.
Results may differ from a plain program's by a relative error of at most 0.015.
The roundings to bfloat16 on the way count: a program that leaves them out, or rounds other values in their place, can miss the bound.
Values may be sent and summed in bfloat16 or wider, within the bound.
A program may use at most 128 MiB of HBM per device.

v0:
```python
import jax
import jax.numpy as jnp
from jax import lax
from jax.experimental import pallas as pl
from jax.experimental.pallas import tpu as pltpu
from jax.sharding import PartitionSpec as P

HEAD = 128
GRID_W = 64


norm_eps = 1e-06
rope_base = 10000.0
clamp_limit = 7.0
sigmoid_slope = 1.702


def rms_scale(values_in, gain):
    return (
        values_in
        * lax.rsqrt(jnp.mean(values_in * values_in, axis=-1, keepdims=True) + norm_eps)
        * gain
    )


def turn_pair(halfpart, cosine, sine):
    first_part, second_part = jnp.split(halfpart, 2, axis=-1)
    return jnp.concatenate(
        [first_part * cosine - second_part * sine, second_part * cosine + first_part * sine],
        axis=-1,
    )


def grid_rotate(field, position):
    half_width = field.shape[-1] // 2
    inverse = rope_base ** (-jnp.arange(0, half_width, 2, dtype=jnp.float32) / half_width)
    grid_row = (position // GRID_W).astype(jnp.float32)
    grid_col = (position % GRID_W).astype(jnp.float32)
    row_angle = (grid_row[:, None] * inverse[None, :])[:, None, :]
    col_angle = (grid_col[:, None] * inverse[None, :])[:, None, :]
    return jnp.concatenate(
        [
            turn_pair(field[..., :half_width], jnp.cos(row_angle), jnp.sin(row_angle)),
            turn_pair(field[..., half_width:], jnp.cos(col_angle), jnp.sin(col_angle)),
        ],
        axis=-1,
    )


def clamped_unit(gate_pre, up_pre):
    gate_cut = jnp.minimum(gate_pre, clamp_limit)
    up_cut = jnp.clip(up_pre, -clamp_limit, clamp_limit)
    return ((up_cut + 1.0) * gate_cut * jax.nn.sigmoid(sigmoid_slope * gate_cut)).astype(
        jnp.bfloat16
    )


def mixer_half(queries, keys, values, query_gain, key_gain, out_weight, mixer_gain):
    local_rows = queries.shape[0]
    kv_local = keys.shape[1] // HEAD
    group_size = queries.shape[1] // HEAD // kv_local
    position = lax.axis_index("ep") * local_rows + jnp.arange(local_rows, dtype=jnp.int32)
    query_f = queries.astype(jnp.float32).reshape(local_rows, kv_local * group_size, HEAD)
    query_norm = grid_rotate(rms_scale(query_f, query_gain), position).astype(jnp.bfloat16)
    query_norm = query_norm.reshape(local_rows, kv_local, group_size, HEAD)
    key_f = keys.astype(jnp.float32).reshape(local_rows, kv_local, HEAD)
    key_norm = grid_rotate(rms_scale(key_f, key_gain), position).astype(jnp.bfloat16)
    key_norm = key_norm.reshape(local_rows, kv_local * HEAD)
    score_scale = HEAD ** (-0.5)
    initial = (
        jnp.full((kv_local, group_size, local_rows), -1e30, jnp.float32),
        jnp.zeros((kv_local, group_size, local_rows), jnp.float32),
        jnp.zeros((kv_local, group_size, local_rows, HEAD), jnp.float32),
    )
    key_piece = lax.all_gather(key_norm, "ep", axis=0, tiled=True)
    value_piece = lax.all_gather(values, "ep", axis=0, tiled=True)
    piece_rows = key_piece.shape[0]
    block_rows = 1
    for candidate in range(min(piece_rows, 1024), 0, -1):
        if piece_rows % candidate == 0:
            block_rows = candidate
            break
    key_blocks = key_piece.reshape(piece_rows // block_rows, block_rows, kv_local, HEAD)
    value_blocks = value_piece.reshape(piece_rows // block_rows, block_rows, kv_local, HEAD)

    def one_block(state, blocks_in):
        running_max, running_total, weighted = state
        key_block, value_block = blocks_in
        scores = (
            jnp.einsum("qhgd,khd->hgqk", query_norm, key_block, preferred_element_type=jnp.float32)
            * score_scale
        )
        new_max = jnp.maximum(running_max, jnp.max(scores, axis=-1))
        factor = jnp.exp(running_max - new_max)
        expo = jnp.exp(scores - new_max[..., None])
        new_total = running_total * factor + jnp.sum(expo, axis=-1)
        new_weighted = weighted * factor[..., None] + jnp.einsum(
            "hgqk,khd->hgqd",
            expo.astype(jnp.bfloat16),
            value_block,
            preferred_element_type=jnp.float32,
        )
        return ((new_max, new_total, new_weighted), None)

    state_out, unused = lax.scan(one_block, initial, (key_blocks, value_blocks))
    final_max, final_total, weighted = state_out
    attended = (weighted / final_total[..., None]).astype(jnp.bfloat16)
    attended = jnp.transpose(attended, (2, 0, 1, 3)).reshape(
        local_rows, kv_local * group_size * HEAD
    )
    share_rows = local_rows // lax.axis_size("tp")
    selected = lax.slice_in_dim(attended, 0, lax.axis_size("tp") * share_rows, axis=0)
    projected = lax.psum_scatter(
        jnp.dot(selected, out_weight, preferred_element_type=jnp.float32).astype(jnp.bfloat16),
        "tp",
        scatter_dimension=0,
        tiled=True,
    ).astype(jnp.float32)
    return rms_scale(projected, mixer_gain).astype(jnp.bfloat16)


def expert_half(expert_in, routes, route_weights, expert_gain, gate_w, up_w, down_w, ffn_out_gain):
    tok_rows = expert_in.shape[0]
    model_width = expert_in.shape[1]
    top_count = routes.shape[1]
    expert_count = lax.axis_size("ep")
    capacity = max(2, (3 * tok_rows * top_count + 2 * expert_count - 1) // (2 * expert_count))
    normed = rms_scale(expert_in.astype(jnp.float32), expert_gain).astype(jnp.bfloat16)
    pair_expert = routes.reshape(-1)
    pair_count = pair_expert.shape[0]
    one_hot = (pair_expert[:, None] == jnp.arange(expert_count, dtype=jnp.int32)[None, :]).astype(
        jnp.int32
    )
    pair_rank = jnp.sum(jnp.cumsum(one_hot, axis=0) * one_hot, axis=1) - 1
    pair_slot = pair_expert * capacity + pair_rank
    slot_pair = (
        jnp.full((expert_count * capacity,), pair_count, jnp.int32)
        .at[pair_slot]
        .set(jnp.arange(pair_count, dtype=jnp.int32))
    )
    padded = jnp.concatenate([normed, jnp.zeros((1, model_width), jnp.bfloat16)], axis=0)
    outgoing = padded[slot_pair // top_count].reshape(expert_count, capacity, model_width)
    gate_local = gate_w[0]
    up_local = up_w[0]
    down_local = down_w[0]
    arrived = lax.all_to_all(outgoing, "ep", split_axis=0, concat_axis=0, tiled=True)
    flat_rows = arrived.reshape(-1, model_width)
    shard_rows = lax.all_gather(flat_rows, "tp", axis=0, tiled=True)
    hidden = clamped_unit(
        jnp.dot(shard_rows, gate_local, preferred_element_type=jnp.float32),
        jnp.dot(shard_rows, up_local, preferred_element_type=jnp.float32),
    )
    selected = lax.slice_in_dim(hidden, 0, lax.axis_size("tp") * flat_rows.shape[0], axis=0)
    result = lax.psum_scatter(
        jnp.dot(selected, down_local, preferred_element_type=jnp.float32).astype(jnp.bfloat16),
        "tp",
        scatter_dimension=0,
        tiled=True,
    )
    finished = result.reshape(arrived.shape)
    returned = lax.all_to_all(finished, "ep", split_axis=0, concat_axis=0, tiled=True)
    pair_result = returned.reshape(-1, model_width)[pair_slot].reshape(
        tok_rows, top_count, model_width
    )
    combined = jnp.einsum("tk,tkd->td", route_weights, pair_result.astype(jnp.float32))
    return rms_scale(combined, ffn_out_gain).astype(jnp.bfloat16)


def flip(index, bits):
    power = 1
    while power <= bits:
        if bits & power:
            index = index + power - 2 * power * lax.rem(lax.div(index, power), 2)
        power *= 2
    return index


def peer_order(count):
    far = [j for j in range(count // 2, count) if j > 1]
    near = [j for j in range(2, count // 2)]
    order = [0, 1]
    while far or near:
        if far:
            order.append(far.pop(0))
        if near:
            order.append(near.pop(0))
    return order[:count]


def capacity_of(tok_rows, top_count, expert_count):
    return max(2, (3 * tok_rows * top_count + 2 * expert_count - 1) // (2 * expert_count))


def fused_fits(queries, keys, expert_in, routes, gate_w):
    n_ep, n_tp = lax.axis_size("ep"), lax.axis_size("tp")
    rows = queries.shape[0]
    capacity = capacity_of(expert_in.shape[0], routes.shape[1], n_ep)
    width = expert_in.shape[1]
    hidden = gate_w.shape[2]
    slots = n_ep * capacity
    held = 2 * width * slots * 14 + 6 * width * hidden * 4 + 4 * rows * rows * n_ep
    return (
        n_tp == 4
        and n_ep >= 4
        and n_ep & (n_ep - 1) == 0
        and keys.shape[1] == HEAD
        and capacity % 16 == 0
        and rows % (16 * n_tp) == 0
        and expert_in.shape[0] % 16 == 0
        and held < 56 * 2**20
    )


def fused_kernel(
    order,
    out_ref_q,
    kv_ref,
    outg_ref,
    weight_ref,
    mixer_gain_ref,
    ffn_gain_ref,
    out_w_hbm,
    gate_hbm,
    up_hbm,
    down_hbm,
    mixer_out_ref,
    expert_out_ref,
    out_w,
    gate,
    up,
    down,
    kv_all,
    att,
    proj,
    proj_in,
    proj_sum,
    proj_xin,
    rows,
    part,
    part_in,
    part_sum,
    part_xin,
    final,
    ret,
    w_sem,
    own_sem,
    kv_send,
    kv_recv,
    disp_send,
    disp_recv,
    core_send,
    core_recv,
    chip_send,
    chip_recv,
    relay_send,
    relay_recv,
    pcore_send,
    pcore_recv,
    pchip_send,
    pchip_recv,
    ret_send,
    ret_recv,
    mix_send,
    mix_recv,
):
    q_ref = out_ref_q
    n = len(order)
    width = rows.shape[1]
    cap = ret.shape[0] // n
    local_rows = kv_ref.shape[0]
    share = local_rows // 4
    heads = q_ref.shape[0] // local_rows
    ep, tp = lax.axis_index("ep"), lax.axis_index("tp")

    def at(ref, start, size):
        return ref.at[pl.ds(start, size), :]

    def remote(src, dst, send, recv, ep_bits, tp_bits):
        return pltpu.make_async_remote_copy(
            src_ref=src,
            dst_ref=dst,
            send_sem=send,
            recv_sem=recv,
            device_id={"ep": flip(ep, ep_bits), "tp": flip(tp, tp_bits)},
            device_id_type=pl.DeviceIdType.MESH,
        )

    loads = [
        pltpu.make_async_copy(a, b, w_sem.at[i])
        for i, (a, b) in enumerate(
            [(gate_hbm, gate), (up_hbm, up), (down_hbm, down), (out_w_hbm, out_w)]
        )
    ]
    for load in loads:
        load.start()
    own_kv = pltpu.make_async_copy(kv_ref, at(kv_all, 0, local_rows), own_sem.at[0])
    own_rows = pltpu.make_async_copy(at(outg_ref, 0, cap), at(rows, 0, cap), own_sem.at[1])
    own_kv.start()
    own_rows.start()

    barrier = pltpu.get_barrier_semaphore()
    peers = [(j, 0) for j in range(1, n)] + [(0, 1), (0, 2)]
    for ep_bits, tp_bits in peers:
        pl.semaphore_signal(
            barrier,
            inc=1,
            device_id={"ep": flip(ep, ep_bits), "tp": flip(tp, tp_bits)},
            device_id_type=pl.DeviceIdType.MESH,
        )
    pl.semaphore_wait(barrier, len(peers))

    kv_stages = []
    held = [0]
    bit = n // 2
    while bit >= 1:
        stage = []
        for block in held:
            source = kv_ref if block == 0 else at(kv_all, block * local_rows, local_rows)
            slot = block + bit
            stage.append(
                remote(
                    source,
                    at(kv_all, slot * local_rows, local_rows),
                    kv_send.at[slot],
                    kv_recv.at[slot],
                    bit,
                    0,
                )
            )
        kv_stages.append(stage)
        held = held + [block + bit for block in held]
        bit //= 2

    def place(slot, which):
        return (4 * slot + which) * cap

    dispatch = [
        None
        if j == 0
        else remote(
            at(outg_ref, k * cap, cap),
            at(rows, place(k, 0), cap),
            disp_send.at[k],
            disp_recv.at[k],
            j,
            0,
        )
        for k, j in enumerate(order)
    ]
    to_core, to_chip, relay = [], [], []
    p_core, p_chip, give_back = [], [], []
    for k, j in enumerate(order):
        source = at(outg_ref, 0, cap) if j == 0 else at(rows, place(k, 0), cap)
        to_core.append(
            remote(source, at(rows, place(k, 2), cap), core_send.at[k], core_recv.at[k], 0, 1)
        )
        to_chip.append(
            remote(source, at(rows, place(k, 1), cap), chip_send.at[k], chip_recv.at[k], 0, 2)
        )
        relay.append(
            remote(
                at(rows, place(k, 1), cap),
                at(rows, place(k, 3), cap),
                relay_send.at[k],
                relay_recv.at[k],
                0,
                1,
            )
        )
        p_core.append(
            remote(
                at(part, place(k, 2), 2 * cap),
                at(part_in, 2 * k * cap, 2 * cap),
                pcore_send.at[k],
                pcore_recv.at[k],
                0,
                1,
            )
        )
        p_chip.append(
            remote(
                at(part_sum, k * cap, cap),
                at(part_xin, k * cap, cap),
                pchip_send.at[k],
                pchip_recv.at[k],
                0,
                2,
            )
        )
        give_back.append(
            None
            if j == 0
            else remote(
                at(final, k * cap, cap),
                at(ret, k * cap, cap),
                ret_send.at[k],
                ret_recv.at[k],
                j,
                0,
            )
        )

    def pair(group):
        return (2 * group, 2 * group + 1)

    def forward_one(k):
        if dispatch[k] is not None:
            dispatch[k].wait_recv()
        to_chip[k].start()
        to_core[k].start()

    def pass_on_one(k):
        to_chip[k].wait_recv()
        relay[k].start()

    def forward(group):
        for k in pair(group):
            forward_one(k)

    def pass_on(group):
        for k in pair(group):
            pass_on_one(k)

    def compute(group):
        for k in pair(group):
            to_core[k].wait_recv()
            relay[k].wait_recv()
        span = pl.ds(place(2 * group, 0), 8 * cap)
        taken = rows[span, :]
        hidden = clamped_unit(
            jnp.dot(taken, gate[...], preferred_element_type=jnp.float32),
            jnp.dot(taken, up[...], preferred_element_type=jnp.float32),
        )
        part[span, :] = jnp.dot(hidden, down[...], preferred_element_type=jnp.float32).astype(
            jnp.bfloat16
        )
        for k in pair(group):
            p_core[k].start()

    def wide(ref, start, size):
        return ref[pl.ds(start, size), :].astype(jnp.float32)

    def reduce_core(group):
        for k in pair(group):
            p_core[k].wait_recv()
            part_sum[pl.ds(k * cap, cap), :] = (
                wide(part, place(k, 1), cap) + wide(part_in, (2 * k + 1) * cap, cap)
            ).astype(jnp.bfloat16)
            p_chip[k].start()

    def reduce_chip(group):
        for k in pair(group):
            p_chip[k].wait_recv()
            summed = (
                wide(part, place(k, 0), cap)
                + wide(part_in, 2 * k * cap, cap)
                + wide(part_xin, k * cap, cap)
            ).astype(jnp.bfloat16)
            if give_back[k] is None:
                ret[pl.ds(k * cap, cap), :] = summed
            else:
                final[pl.ds(k * cap, cap), :] = summed
                give_back[k].start()

    def attend(head):
        query = q_ref[pl.ds(head * local_rows, local_rows), :]
        scores = lax.dot_general(
            query,
            kv_all[:, :HEAD],
            (((1,), (1,)), ((), ())),
            preferred_element_type=jnp.float32,
        ) * (HEAD ** (-0.5))
        expo = jnp.exp(scores - jnp.max(scores, axis=-1, keepdims=True))
        total = jnp.sum(expo, axis=-1, keepdims=True)
        summed = jnp.dot(
            expo.astype(jnp.bfloat16), kv_all[:, HEAD:], preferred_element_type=jnp.float32
        )
        att[:, head * HEAD : (head + 1) * HEAD] = (summed / total).astype(jnp.bfloat16)

    def block_of(bits):
        return pl.multiple_of(flip(tp, bits) * share, share)

    mix_core = [
        remote(
            at(proj, block_of(1), share),
            at(proj_in, 0, share),
            mix_send.at[0],
            mix_recv.at[0],
            0,
            1,
        ),
        remote(
            at(proj, block_of(3), share),
            at(proj_in, share, share),
            mix_send.at[1],
            mix_recv.at[1],
            0,
            1,
        ),
    ]
    mix_chip = remote(proj_sum, proj_xin, mix_send.at[2], mix_recv.at[2], 0, 2)

    def project():
        proj[...] = jnp.dot(att[...], out_w[...], preferred_element_type=jnp.float32).astype(
            jnp.bfloat16
        )
        for copy in mix_core:
            copy.start()

    def mix_reduce():
        for copy in mix_core:
            copy.wait_recv()
        proj_sum[...] = (wide(proj, block_of(2), share) + wide(proj_in, share, share)).astype(
            jnp.bfloat16
        )
        mix_chip.start()

    def mix_finish():
        mix_chip.wait_recv()
        summed = (
            wide(proj, block_of(0), share)
            + wide(proj_in, 0, share)
            + proj_xin[...].astype(jnp.float32)
        )
        mixer_out_ref[...] = rms_scale(summed, mixer_gain_ref[...]).astype(jnp.bfloat16)

    groups = n // 2
    for copy in kv_stages[0]:
        copy.start()
    dispatch[1].start()
    for k in range(2, 4):
        dispatch[k].start()
    forward_one(0)
    forward_one(1)
    for copies, later in zip(kv_stages[:-1], kv_stages[1:]):
        for copy in copies:
            copy.wait_recv()
        for copy in later:
            copy.start()
        if copies is kv_stages[0]:
            for k in range(4, n):
                dispatch[k].start()
            own_rows.wait()
            pass_on(0)
            for load in loads[:3]:
                load.wait()
            compute(0)
            forward(1)
            reduce_core(0)
    pass_on(1)
    own_kv.wait()
    for copy in kv_stages[-1]:
        copy.wait_recv()
    for group in range(1, groups):
        if group + 1 < groups:
            forward(group + 1)
        compute(group)
        if group < 2:
            reduce_chip(group - 1)
        if group + 1 < groups:
            pass_on(group + 1)
        if group == 1:
            for head in range(heads // 2):
                attend(head)
        reduce_core(group)
        if group >= 2:
            reduce_chip(group - 1)
        if group == 1:
            for head in range(heads // 2, heads):
                attend(head)
            loads[3].wait()
            project()
        if group == 2:
            mix_reduce()
    mix_finish()
    reduce_chip(groups - 1)
    for copy in give_back:
        if copy is not None:
            copy.wait_recv()

    rest = weight_ref[...]
    combined = jnp.zeros((weight_ref.shape[0], width), jnp.float32)
    for _ in range(3):
        piece = rest.astype(jnp.bfloat16)
        rest = rest - piece.astype(jnp.float32)
        combined = combined + jnp.dot(piece, ret[...], preferred_element_type=jnp.float32)
    expert_out_ref[...] = rms_scale(combined, ffn_gain_ref[...]).astype(jnp.bfloat16)

    for copy in (
        [c for stage in kv_stages for c in stage]
        + dispatch
        + to_core
        + to_chip
        + relay
        + p_core
        + p_chip
        + give_back
        + mix_core
        + [mix_chip]
    ):
        if copy is not None:
            copy.wait_send()


def fused_local(
    queries,
    keys,
    values,
    query_gain,
    key_gain,
    out_weight,
    mixer_gain,
    expert_in,
    routes,
    route_weights,
    expert_gain,
    gate_w,
    up_w,
    down_w,
    ffn_out_gain,
):
    n = lax.axis_size("ep")
    order = peer_order(n)
    local_rows = queries.shape[0]
    heads = queries.shape[1] // HEAD
    tok_rows, width = expert_in.shape
    cap = capacity_of(tok_rows, routes.shape[1], n)
    hidden = gate_w.shape[2]
    share = local_rows // 4
    ep = lax.axis_index("ep")

    position = ep * local_rows + jnp.arange(local_rows, dtype=jnp.int32)
    both = jnp.concatenate([queries, keys], axis=1).astype(jnp.float32)
    both = both.reshape(local_rows, heads + 1, HEAD)
    gains = jnp.concatenate(
        [jnp.broadcast_to(query_gain, (heads, HEAD)), key_gain[None]], axis=0
    )
    turned = grid_rotate(rms_scale(both, gains), position).astype(jnp.bfloat16)
    query_norm = jnp.transpose(turned[:, :heads], (1, 0, 2)).reshape(heads * local_rows, HEAD)
    key_value = jnp.concatenate([turned[:, heads], values], axis=1)

    normed = rms_scale(expert_in.astype(jnp.float32), expert_gain).astype(jnp.bfloat16)
    slot_expert = jnp.bitwise_xor(ep.astype(jnp.int32), jnp.array(order, jnp.int32))
    named = routes[:, :, None] == slot_expert[None, None, :]
    chosen = jnp.any(named, axis=1)
    weight = jnp.sum(jnp.where(named, route_weights[:, :, None], 0.0), axis=1)
    token = jnp.arange(tok_rows, dtype=jnp.int32)
    earlier = (token[:, None] > token[None, :]).astype(jnp.bfloat16)
    rank = jnp.dot(earlier, chosen.astype(jnp.bfloat16), preferred_element_type=jnp.float32)
    rank = rank.astype(jnp.int32)
    taken = chosen[:, :, None] & (rank[:, :, None] == jnp.arange(cap, dtype=jnp.int32))
    slot_weight = jnp.where(taken, weight[:, :, None], 0.0).reshape(tok_rows, n * cap)
    pick = taken.astype(jnp.bfloat16).reshape(tok_rows, n * cap)
    outgoing = lax.dot_general(
        pick, normed, (((0,), (0,)), ((), ())), preferred_element_type=jnp.float32
    ).astype(jnp.bfloat16)

    vmem = pl.BlockSpec(memory_space=pltpu.VMEM)
    anywhere = pl.BlockSpec(memory_space=pl.ANY)
    bf16 = jnp.bfloat16
    dma = pltpu.SemaphoreType.DMA

    def fused(*refs):
        return fused_kernel(order, *refs)

    return pl.pallas_call(
        fused,
        out_shape=(
            jax.ShapeDtypeStruct((share, width), bf16),
            jax.ShapeDtypeStruct((tok_rows, width), bf16),
        ),
        in_specs=[vmem] * 6 + [anywhere] * 4,
        out_specs=(vmem, vmem),
        scratch_shapes=[
            pltpu.VMEM((heads * HEAD, width), bf16),
            pltpu.VMEM((width, hidden), bf16),
            pltpu.VMEM((width, hidden), bf16),
            pltpu.VMEM((hidden, width), bf16),
            pltpu.VMEM((n * local_rows, 2 * HEAD), bf16),
            pltpu.VMEM((local_rows, heads * HEAD), bf16),
            pltpu.VMEM((local_rows, width), bf16),
            pltpu.VMEM((2 * share, width), bf16),
            pltpu.VMEM((share, width), bf16),
            pltpu.VMEM((share, width), bf16),
            pltpu.VMEM((4 * n * cap, width), bf16),
            pltpu.VMEM((4 * n * cap, width), bf16),
            pltpu.VMEM((2 * n * cap, width), bf16),
            pltpu.VMEM((n * cap, width), bf16),
            pltpu.VMEM((n * cap, width), bf16),
            pltpu.VMEM((n * cap, width), bf16),
            pltpu.VMEM((n * cap, width), bf16),
            dma((4,)),
            dma((2,)),
        ]
        + [dma((n,))] * 16
        + [dma((3,))] * 2,
        compiler_params=pltpu.CompilerParams(
            collective_id=0, has_side_effects=True, vmem_limit_bytes=60 * 2**20
        ),
    )(
        query_norm,
        key_value,
        outgoing,
        slot_weight,
        mixer_gain[None],
        ffn_out_gain[None],
        out_weight,
        gate_w[0],
        up_w[0],
        down_w[0],
    )


def local(
    queries,
    keys,
    values,
    query_gain,
    key_gain,
    out_weight,
    mixer_gain,
    expert_in,
    routes,
    route_weights,
    expert_gain,
    gate_w,
    up_w,
    down_w,
    ffn_out_gain,
):
    if fused_fits(queries, keys, expert_in, routes, gate_w):
        return fused_local(
            queries, keys, values, query_gain, key_gain, out_weight, mixer_gain, expert_in, routes,
            route_weights, expert_gain, gate_w, up_w, down_w, ffn_out_gain,
        )
    mixer_out = mixer_half(queries, keys, values, query_gain, key_gain, out_weight, mixer_gain)
    expert_out = expert_half(
        expert_in, routes, route_weights, expert_gain, gate_w, up_w, down_w, ffn_out_gain
    )
    return (mixer_out, expert_out)


def solution(mesh):
    in_specs = (
        P("ep", "tp"),
        P("ep", "tp"),
        P("ep", "tp"),
        P(),
        P(),
        P("tp", None),
        P(),
        P(("ep", "tp"), None),
        P(("ep", "tp"), None),
        P(("ep", "tp"), None),
        P(),
        P("ep", None, "tp"),
        P("ep", None, "tp"),
        P("ep", "tp", None),
        P(),
    )
    out_specs = (P(("ep", "tp"), None), P(("ep", "tp"), None))
    return jax.shard_map(local, mesh=mesh, in_specs=in_specs, out_specs=out_specs, check_vma=False)
```

profile of v0, /device:TPU:9, one launch (start us, length us, event | category | flops | bytes accessed | tf_op | source)
XLA Modules:
  0.0 122.8 jit_solution(13774342254487313109)
XLA Ops:
  0.6 0.0 copy-start.2
  0.6 0.0 copy-start.1
  0.7 0.7 broadcast_xor_fusion
  1.4 1.2 fusion
  2.6 0.8 compare_reduce_fusion
  3.4 0.7 broadcast_in_dim.30
  4.0 0.7 pad_maximum_fusion.2
  4.7 0.8 fusion.6
  5.5 0.1 convolution_convert_fusion.1
  5.6 0.1 eq.42
  5.7 0.1 copy.31
  5.9 0.1 copy.30
  6.1 0.1 copy.32
  6.2 0.7 broadcast_select_fusion
  6.9 0.8 multiply_cosine_fusion.1
  7.7 0.0 copy-done.2
  7.7 0.0 copy-done.1
  7.8 0.2 copy.28
  8.0 0.1 multiply_reduce_fusion
  8.1 0.2 copy.29
  8.3 0.2 multiply_multiply_fusion
  8.5 0.5 subtract_convert_fusion.1
  9.0 0.0 copy-start.3
  9.0 0.0 copy-start
  9.0 0.0 copy-start.4
  9.0 0.1 maximum_bitcast_fusion
  9.1 0.3 pad_maximum_fusion
  9.5 0.7 slice.14
  10.2 0.0 copy-done.3
  10.2 0.6 pad_maximum_fusion.1.refs_1_
  10.8 0.0 copy-done
  10.8 0.0 copy-done.4
  10.8 1.8 %convolution_convert_fusion.refs_2_ = bf16[384,2048]{1,0:T(8,128)(2,1)} fusion(pred[128,384]{1,0:T(32,128)(4,1)S(1)} %get-tuple-element.3, bf16[128,2048]{1,0:T(8,128)(2,1)S(1)} %copy-done, f32[2048]{0:T(1024)S(1)} %copy-done.4, f32[128]{0:T(128)S(1)} %add_rsqrt_fusion.1), kind=kOutput, calls=%fused_computation | convolution fusion | flops 203161600 | bytes 2155008 | tf_op jit(solution)/shard_map/dot_general | solution.py:654
  12.6 106.7 %shard_map.167 = (bf16[48,2048]{1,0:T(8,128)(2,1)}, bf16[128,2048]{1,0:T(8,128)(2,1)}) custom-call(bf16[768,128]{1,0:T(8,128)(2,1)} %bitcast.24, bf16[192,256]{1,0:T(8,128)(2,1)} %pad_maximum_fusion.1.refs_1_, bf16[384,2048]{1,0:T(8,128)(2,1)} %convolution_convert_fusion.refs_2_, f32[128,384]{1,0:T(8,128)} %get-tuple-element.2.refs_3_, f32[1,2048]{1,0:T(1,128)} %bitcast.26, ...), custom_call_target="tpu_custom_call" | custom-call | tf_op jit(solution)/shard_map/pallas_call | solution.py:666
  119.3 1.6 %copy.38 = bf16[48,2048]{1,0:T(8,128)(2,1)} copy(bf16[48,2048]{1,0:T(8,128)(2,1)} %get-tuple-element.20) | data formatting | bytes 393216
  120.9 1.9 %copy.39 = bf16[128,2048]{1,0:T(8,128)(2,1)} copy(bf16[128,2048]{1,0:T(8,128)(2,1)} %get-tuple-element.21) | data formatting | bytes 1048576
  (9 shorter events, 0.1 us)
Async XLA Ops:
  0.6 7.1 %copy-start.2 = (bf16[192,128]{1,0:T(8,128)(2,1)S(1)}, bf16[192,128]{1,0:T(8,128)(2,1)}, u32[]{:S(2)}) copy-start(bf16[192,128]{1,0:T(8,128)(2,1)} %param.17) | copy-start | bytes 147460
  0.6 7.1 %copy-start.1 = (bf16[192,512]{1,0:T(8,128)(2,1)S(1)}, bf16[192,512]{1,0:T(8,128)(2,1)}, u32[]{:S(2)}) copy-start(bf16[192,512]{1,0:T(8,128)(2,1)} %param.16) | copy-start | bytes 589828
  9.0 1.2 copy-start.3
  9.0 1.8 %copy-start = (bf16[128,2048]{1,0:T(8,128)(2,1)S(1)}, bf16[128,2048]{1,0:T(8,128)(2,1)}, u32[]{:S(2)}) copy-start(bf16[128,2048]{1,0:T(8,128)(2,1)} %param.23) | copy-start | bytes 1572868
  9.0 1.8 %copy-start.4 = (f32[2048]{0:T(1024)S(1)}, f32[2048]{0:T(1024)}, u32[]{:S(2)}) copy-start(f32[2048]{0:T(1024)} %param.26) | copy-start | bytes 24580
where the time goes:
time: 123 us
  Pallas kernels  107 us (87%)
  other arithmetic  7.51 us (6%)
  local copies, waits for them, and re-layouts  5.87 us (5%)
  matrix products  1.96 us (2%)
    pallas_call x1, Pallas kernels, fused_local(): pl.pallas_call(fused, out_shape=(jax.ShapeDtypeStruct((share, width), bf1...  107 us
    unnamed x12, local copies, waits for them, and re-layouts  3.52 us

commit v1 on v0

v1 whole, which is shorter than its diff:
```python
import jax
import jax.numpy as jnp
import numpy as np
from jax import lax
from jax.experimental import pallas as pl
from jax.experimental.pallas import tpu as pltpu
from jax.sharding import PartitionSpec as P

HEAD = 128
GRID_W = 64


norm_eps = 1e-06
rope_base = 10000.0
clamp_limit = 7.0
sigmoid_slope = 1.702


def rms_scale(values_in, gain):
    return (
        values_in
        * lax.rsqrt(jnp.mean(values_in * values_in, axis=-1, keepdims=True) + norm_eps)
        * gain
    )


def turn_pair(halfpart, cosine, sine):
    first_part, second_part = jnp.split(halfpart, 2, axis=-1)
    return jnp.concatenate(
        [first_part * cosine - second_part * sine, second_part * cosine + first_part * sine],
        axis=-1,
    )


def grid_rotate(field, position):
    half_width = field.shape[-1] // 2
    inverse = rope_base ** (-jnp.arange(0, half_width, 2, dtype=jnp.float32) / half_width)
    grid_row = (position // GRID_W).astype(jnp.float32)
    grid_col = (position % GRID_W).astype(jnp.float32)
    row_angle = (grid_row[:, None] * inverse[None, :])[:, None, :]
    col_angle = (grid_col[:, None] * inverse[None, :])[:, None, :]
    return jnp.concatenate(
        [
            turn_pair(field[..., :half_width], jnp.cos(row_angle), jnp.sin(row_angle)),
            turn_pair(field[..., half_width:], jnp.cos(col_angle), jnp.sin(col_angle)),
        ],
        axis=-1,
    )


def clamped_unit(gate_pre, up_pre):
    gate_cut = jnp.minimum(gate_pre, clamp_limit)
    up_cut = jnp.clip(up_pre, -clamp_limit, clamp_limit)
    return ((up_cut + 1.0) * gate_cut * jax.nn.sigmoid(sigmoid_slope * gate_cut)).astype(
        jnp.bfloat16
    )


def mixer_half(queries, keys, values, query_gain, key_gain, out_weight, mixer_gain):
    local_rows = queries.shape[0]
    kv_local = keys.shape[1] // HEAD
    group_size = queries.shape[1] // HEAD // kv_local
    position = lax.axis_index("ep") * local_rows + jnp.arange(local_rows, dtype=jnp.int32)
    query_f = queries.astype(jnp.float32).reshape(local_rows, kv_local * group_size, HEAD)
    query_norm = grid_rotate(rms_scale(query_f, query_gain), position).astype(jnp.bfloat16)
    query_norm = query_norm.reshape(local_rows, kv_local, group_size, HEAD)
    key_f = keys.astype(jnp.float32).reshape(local_rows, kv_local, HEAD)
    key_norm = grid_rotate(rms_scale(key_f, key_gain), position).astype(jnp.bfloat16)
    key_norm = key_norm.reshape(local_rows, kv_local * HEAD)
    score_scale = HEAD ** (-0.5)
    initial = (
        jnp.full((kv_local, group_size, local_rows), -1e30, jnp.float32),
        jnp.zeros((kv_local, group_size, local_rows), jnp.float32),
        jnp.zeros((kv_local, group_size, local_rows, HEAD), jnp.float32),
    )
    key_piece = lax.all_gather(key_norm, "ep", axis=0, tiled=True)
    value_piece = lax.all_gather(values, "ep", axis=0, tiled=True)
    piece_rows = key_piece.shape[0]
    block_rows = 1
    for candidate in range(min(piece_rows, 1024), 0, -1):
        if piece_rows % candidate == 0:
            block_rows = candidate
            break
    key_blocks = key_piece.reshape(piece_rows // block_rows, block_rows, kv_local, HEAD)
    value_blocks = value_piece.reshape(piece_rows // block_rows, block_rows, kv_local, HEAD)

    def one_block(state, blocks_in):
        running_max, running_total, weighted = state
        key_block, value_block = blocks_in
        scores = (
            jnp.einsum("qhgd,khd->hgqk", query_norm, key_block, preferred_element_type=jnp.float32)
            * score_scale
        )
        new_max = jnp.maximum(running_max, jnp.max(scores, axis=-1))
        factor = jnp.exp(running_max - new_max)
        expo = jnp.exp(scores - new_max[..., None])
        new_total = running_total * factor + jnp.sum(expo, axis=-1)
        new_weighted = weighted * factor[..., None] + jnp.einsum(
            "hgqk,khd->hgqd",
            expo.astype(jnp.bfloat16),
            value_block,
            preferred_element_type=jnp.float32,
        )
        return ((new_max, new_total, new_weighted), None)

    state_out, unused = lax.scan(one_block, initial, (key_blocks, value_blocks))
    final_max, final_total, weighted = state_out
    attended = (weighted / final_total[..., None]).astype(jnp.bfloat16)
    attended = jnp.transpose(attended, (2, 0, 1, 3)).reshape(
        local_rows, kv_local * group_size * HEAD
    )
    share_rows = local_rows // lax.axis_size("tp")
    selected = lax.slice_in_dim(attended, 0, lax.axis_size("tp") * share_rows, axis=0)
    projected = lax.psum_scatter(
        jnp.dot(selected, out_weight, preferred_element_type=jnp.float32).astype(jnp.bfloat16),
        "tp",
        scatter_dimension=0,
        tiled=True,
    ).astype(jnp.float32)
    return rms_scale(projected, mixer_gain).astype(jnp.bfloat16)


def expert_half(expert_in, routes, route_weights, expert_gain, gate_w, up_w, down_w, ffn_out_gain):
    tok_rows = expert_in.shape[0]
    model_width = expert_in.shape[1]
    top_count = routes.shape[1]
    expert_count = lax.axis_size("ep")
    capacity = max(2, (3 * tok_rows * top_count + 2 * expert_count - 1) // (2 * expert_count))
    normed = rms_scale(expert_in.astype(jnp.float32), expert_gain).astype(jnp.bfloat16)
    pair_expert = routes.reshape(-1)
    pair_count = pair_expert.shape[0]
    one_hot = (pair_expert[:, None] == jnp.arange(expert_count, dtype=jnp.int32)[None, :]).astype(
        jnp.int32
    )
    pair_rank = jnp.sum(jnp.cumsum(one_hot, axis=0) * one_hot, axis=1) - 1
    pair_slot = pair_expert * capacity + pair_rank
    slot_pair = (
        jnp.full((expert_count * capacity,), pair_count, jnp.int32)
        .at[pair_slot]
        .set(jnp.arange(pair_count, dtype=jnp.int32))
    )
    padded = jnp.concatenate([normed, jnp.zeros((1, model_width), jnp.bfloat16)], axis=0)
    outgoing = padded[slot_pair // top_count].reshape(expert_count, capacity, model_width)
    gate_local = gate_w[0]
    up_local = up_w[0]
    down_local = down_w[0]
    arrived = lax.all_to_all(outgoing, "ep", split_axis=0, concat_axis=0, tiled=True)
    flat_rows = arrived.reshape(-1, model_width)
    shard_rows = lax.all_gather(flat_rows, "tp", axis=0, tiled=True)
    hidden = clamped_unit(
        jnp.dot(shard_rows, gate_local, preferred_element_type=jnp.float32),
        jnp.dot(shard_rows, up_local, preferred_element_type=jnp.float32),
    )
    selected = lax.slice_in_dim(hidden, 0, lax.axis_size("tp") * flat_rows.shape[0], axis=0)
    result = lax.psum_scatter(
        jnp.dot(selected, down_local, preferred_element_type=jnp.float32).astype(jnp.bfloat16),
        "tp",
        scatter_dimension=0,
        tiled=True,
    )
    finished = result.reshape(arrived.shape)
    returned = lax.all_to_all(finished, "ep", split_axis=0, concat_axis=0, tiled=True)
    pair_result = returned.reshape(-1, model_width)[pair_slot].reshape(
        tok_rows, top_count, model_width
    )
    combined = jnp.einsum("tk,tkd->td", route_weights, pair_result.astype(jnp.float32))
    return rms_scale(combined, ffn_out_gain).astype(jnp.bfloat16)


def flip(index, bits):
    power = 1
    while power <= bits:
        if bits & power:
            index = index + power - 2 * power * lax.rem(lax.div(index, power), 2)
        power *= 2
    return index


def capacity_of(tok_rows, top_count, expert_count):
    return max(2, (3 * tok_rows * top_count + 2 * expert_count - 1) // (2 * expert_count))


def fused_fits(queries, keys, expert_in, routes, gate_w):
    n_ep, n_tp = lax.axis_size("ep"), lax.axis_size("tp")
    rows = queries.shape[0]
    capacity = capacity_of(expert_in.shape[0], routes.shape[1], n_ep)
    width = expert_in.shape[1]
    hidden = gate_w.shape[2]
    slots = n_ep * capacity
    held = 2 * width * slots * 14 + 6 * width * hidden * 4 + 4 * rows * rows * n_ep
    return (
        n_tp == 4
        and n_ep >= 4
        and n_ep & (n_ep - 1) == 0
        and keys.shape[1] == HEAD
        and capacity % 16 == 0
        and rows % (16 * n_tp) == 0
        and rows % GRID_W == 0
        and queries.shape[1] % HEAD == 0
        and expert_in.shape[0] % 16 == 0
        and held < 56 * 2**20
    )


STEPS = (
    "F0", "D2", "W", "D1", "KR", "D3", "K0", "F1", "D4", "F2", "F3", "R2", "R1", "R0", "D6",
    "C2", "F4", "P2", "R3", "K1", "D5", "R4", "F6", "C4", "P4", "C1", "D7", "R6", "G2", "C3",
    "P1", "G4", "K2", "F5", "C6", "P6", "G1", "F7", "R5", "C5", "G6", "P5", "P3", "R7", "C7",
    "G5", "C0", "P7", "A0", "A1", "A2", "G3", "P0", "A3", "O", "M", "G7", "G0", "N", "E",
)


def rope_tables(grid_rows):
    half = HEAD // 2
    lane = np.arange(HEAD)
    inverse = rope_base ** (-2.0 * (lane % (half // 2)) / half)
    sign = np.where(lane % half < half // 2, -1.0, 1.0)
    row = np.arange(grid_rows)[:, None] * inverse[None, :]
    col = np.arange(GRID_W)[:, None] * inverse[None, :]
    low = (lane < half)[None, :]
    tables = (
        np.where(low, np.cos(row), 0.0),
        np.where(low, np.sin(row) * sign, 0.0),
        np.where(low, 0.0, np.cos(col)),
        np.where(low, 0.0, np.sin(col) * sign),
    )
    return [jnp.asarray(t.astype(np.float32)) for t in tables]


def fused_kernel(
    query_hbm,
    key_hbm,
    value_hbm,
    expert_hbm,
    out_w_hbm,
    gate_hbm,
    up_hbm,
    down_hbm,
    query_gain_ref,
    key_gain_ref,
    mixer_gain_ref,
    expert_gain_ref,
    ffn_gain_ref,
    routes_ref,
    route_weight_ref,
    row_cos_ref,
    row_sin_ref,
    col_cos_ref,
    col_sin_ref,
    mixer_out_ref,
    expert_out_ref,
    query,
    key,
    expert_in,
    out_w,
    gate,
    up,
    down,
    kv_all,
    att,
    proj,
    proj_in,
    proj_sum,
    proj_xin,
    outg,
    slot_weight,
    rows,
    part,
    part_in,
    part_sum,
    part_xin,
    final,
    ret,
    load_sem,
    kv_send,
    kv_recv,
    disp_send,
    disp_recv,
    core_send,
    core_recv,
    chip_send,
    chip_recv,
    relay_send,
    relay_recv,
    pcore_send,
    pcore_recv,
    pchip_send,
    pchip_recv,
    ret_send,
    ret_recv,
    mix_send,
    mix_recv,
):
    tok_rows, width = expert_in.shape
    n = disp_send.shape[0]
    cap = ret.shape[0] // n
    local_rows = key.shape[0]
    share = local_rows // 4
    heads = query.shape[1] // HEAD
    grid_rows = local_rows // GRID_W
    bf16, f32 = jnp.bfloat16, jnp.float32
    ep, tp = lax.axis_index("ep"), lax.axis_index("tp")

    def at(ref, start, size):
        return ref.at[pl.ds(start, size), :]

    def remote(src, dst, send, recv, ep_bits, tp_bits):
        return pltpu.make_async_remote_copy(
            src_ref=src,
            dst_ref=dst,
            send_sem=send,
            recv_sem=recv,
            device_id={"ep": flip(ep, ep_bits), "tp": flip(tp, tp_bits)},
            device_id_type=pl.DeviceIdType.MESH,
        )

    loads = {
        name: pltpu.make_async_copy(a, b, load_sem.at[i])
        for i, (name, a, b) in enumerate(
            [
                ("expert", expert_hbm, expert_in),
                ("key", key_hbm, key),
                ("value", value_hbm, kv_all.at[pl.ds(0, local_rows), pl.ds(HEAD, HEAD)]),
                ("query", query_hbm, query),
                ("gate", gate_hbm, gate),
                ("up", up_hbm, up),
                ("down", down_hbm, down),
                ("out", out_w_hbm, out_w),
            ]
        )
    }
    for load in loads.values():
        load.start()

    def settle(name):
        if name in loads:
            loads.pop(name).wait()

    barrier = pltpu.get_barrier_semaphore()
    peers = [(j, 0) for j in range(1, n)] + [(0, 1), (0, 2)]
    for ep_bits, tp_bits in peers:
        pl.semaphore_signal(
            barrier,
            inc=1,
            device_id={"ep": flip(ep, ep_bits), "tp": flip(tp, tp_bits)},
            device_id_type=pl.DeviceIdType.MESH,
        )

    kv_stages = []
    held = [0]
    bit = n // 2
    while bit >= 1:
        kv_stages.append(
            [
                remote(
                    at(kv_all, block * local_rows, local_rows),
                    at(kv_all, (block + bit) * local_rows, local_rows),
                    kv_send.at[block + bit],
                    kv_recv.at[block + bit],
                    bit,
                    0,
                )
                for block in held
            ]
        )
        held = held + [block + bit for block in held]
        bit //= 2

    kv_last = list(kv_stages[-1])

    def place(slot, which):
        return (4 * slot + which) * cap

    dispatch, to_core, to_chip, relay = [], [], [], []
    p_core, p_chip, give_back = [], [], []
    for j in range(n):
        own = at(rows, place(j, 0), cap)
        dispatch.append(
            None
            if j == 0
            else remote(at(outg, j * cap, cap), own, disp_send.at[j], disp_recv.at[j], j, 0)
        )
        to_core.append(
            remote(own, at(rows, place(j, 2), cap), core_send.at[j], core_recv.at[j], 0, 1)
        )
        to_chip.append(
            remote(own, at(rows, place(j, 1), cap), chip_send.at[j], chip_recv.at[j], 0, 2)
        )
        relay.append(
            remote(
                at(rows, place(j, 1), cap),
                at(rows, place(j, 3), cap),
                relay_send.at[j],
                relay_recv.at[j],
                0,
                1,
            )
        )
        p_core.append(
            remote(
                at(part, place(j, 2), 2 * cap),
                at(part_in, 2 * j * cap, 2 * cap),
                pcore_send.at[j],
                pcore_recv.at[j],
                0,
                1,
            )
        )
        p_chip.append(
            remote(
                at(part_sum, j * cap, cap),
                at(part_xin, j * cap, cap),
                pchip_send.at[j],
                pchip_recv.at[j],
                0,
                2,
            )
        )
        give_back.append(
            None
            if j == 0
            else remote(
                at(final, j * cap, cap),
                at(ret, j * cap, cap),
                ret_send.at[j],
                ret_recv.at[j],
                j,
                0,
            )
        )

    def route():
        settle("expert")
        normed = rms_scale(expert_in[...].astype(f32), expert_gain_ref[...]).astype(bf16)
        number = lax.broadcasted_iota(jnp.int32, (n, tok_rows), 0)
        number = jnp.bitwise_xor(number, ep.astype(jnp.int32))
        chosen = jnp.zeros((n, tok_rows), f32)
        weight = jnp.zeros((n, tok_rows), f32)
        for k in range(routes_ref.shape[0]):
            same = routes_ref[k : k + 1, :] == number
            chosen = jnp.where(same, 1.0, chosen)
            weight = jnp.where(same, route_weight_ref[k : k + 1, :], weight)
        earlier = (
            lax.broadcasted_iota(jnp.int32, (tok_rows, tok_rows), 0)
            < lax.broadcasted_iota(jnp.int32, (tok_rows, tok_rows), 1)
        ).astype(f32)
        rank = jnp.dot(chosen, earlier, preferred_element_type=f32)
        rank = jnp.where(chosen > 0.5, rank, -1.0)
        slot = lax.broadcasted_iota(jnp.int32, (cap, tok_rows), 0).astype(f32)
        picks = []
        for j in range(n):
            taken = slot == rank[j : j + 1, :]
            picks.append(jnp.where(taken, 1.0, 0.0))
            slot_weight[j * cap : (j + 1) * cap, :] = jnp.where(taken, weight[j : j + 1, :], 0.0)
        pick = jnp.concatenate(picks, axis=0).astype(bf16)
        out = jnp.dot(pick, normed, preferred_element_type=f32).astype(bf16)
        rows[0:cap, :] = out[0:cap, :]
        outg[cap:, :] = out[cap:, :]

    def turned(values_in, gain):
        field = rms_scale(values_in.astype(f32), gain)
        lane = lax.broadcasted_iota(jnp.int32, field.shape, 1)
        first = jnp.bitwise_and(lane, HEAD // 2 - 1) < HEAD // 4
        partner = jnp.where(
            first,
            pltpu.roll(field, HEAD - HEAD // 4, axis=1),
            pltpu.roll(field, HEAD // 4, axis=1),
        )
        pieces = []
        for r in range(grid_rows):
            span = slice(r * GRID_W, (r + 1) * GRID_W)
            line = pl.ds(ep * grid_rows + r, 1)
            cosine = row_cos_ref[line, :] + col_cos_ref[...]
            sine = row_sin_ref[line, :] + col_sin_ref[...]
            pieces.append(field[span] * cosine + partner[span] * sine)
        return jnp.concatenate(pieces, axis=0).astype(bf16)

    def turn_keys():
        settle("key")
        kv_all[0:local_rows, 0:HEAD] = turned(key[...], key_gain_ref[...])
        settle("value")

    def forward(j):
        if j:
            dispatch[j].wait_recv()
        to_chip[j].start()
        to_core[j].start()

    def pass_on(j):
        to_chip[j].wait_recv()
        relay[j].start()

    def compute(js):
        for name in ("gate", "up", "down"):
            settle(name)
        for j in js:
            to_core[j].wait_recv()
            relay[j].wait_recv()
        span = pl.ds(place(js[0], 0), 4 * len(js) * cap)
        taken = rows[span, :]
        hidden = clamped_unit(
            jnp.dot(taken, gate[...], preferred_element_type=f32),
            jnp.dot(taken, up[...], preferred_element_type=f32),
        )
        part[span, :] = jnp.dot(hidden, down[...], preferred_element_type=f32).astype(bf16)
        for j in js:
            p_core[j].start()

    def wide(ref, start, size):
        return ref[pl.ds(start, size), :].astype(f32)

    def reduce_core(j):
        p_core[j].wait_recv()
        part_sum[pl.ds(j * cap, cap), :] = (
            wide(part, place(j, 1), cap) + wide(part_in, (2 * j + 1) * cap, cap)
        ).astype(bf16)
        p_chip[j].start()

    def reduce_chip(j):
        p_chip[j].wait_recv()
        summed = (
            wide(part, place(j, 0), cap)
            + wide(part_in, 2 * j * cap, cap)
            + wide(part_xin, j * cap, cap)
        ).astype(bf16)
        if j == 0:
            ret[pl.ds(0, cap), :] = summed
        else:
            final[pl.ds(j * cap, cap), :] = summed
            give_back[j].start()

    def kv_stage(s):
        if s:
            for copy in kv_stages[s - 1]:
                copy.wait_recv()
        for copy in kv_stages[s]:
            copy.start()

    def attend(head):
        settle("query")
        while kv_last:
            kv_last.pop().wait_recv()
        column = slice(head * HEAD, (head + 1) * HEAD)
        scores = lax.dot_general(
            turned(query[:, column], query_gain_ref[...]),
            kv_all[:, :HEAD],
            (((1,), (1,)), ((), ())),
            preferred_element_type=f32,
        ) * (HEAD ** (-0.5))
        expo = jnp.exp(scores - jnp.max(scores, axis=-1, keepdims=True))
        total = jnp.sum(expo, axis=-1, keepdims=True)
        summed = jnp.dot(expo.astype(bf16), kv_all[:, HEAD:], preferred_element_type=f32)
        att[:, column] = (summed / total).astype(bf16)

    def block_of(bits):
        return pl.multiple_of(flip(tp, bits) * share, share)

    mix_core = [
        remote(
            at(proj, block_of(1 + 2 * i), share),
            at(proj_in, i * share, share),
            mix_send.at[i],
            mix_recv.at[i],
            0,
            1,
        )
        for i in range(2)
    ]
    mix_chip = remote(proj_sum, proj_xin, mix_send.at[2], mix_recv.at[2], 0, 2)

    def project():
        settle("out")
        proj[...] = jnp.dot(att[...], out_w[...], preferred_element_type=f32).astype(bf16)
        for copy in mix_core:
            copy.start()

    def mix_reduce():
        for copy in mix_core:
            copy.wait_recv()
        proj_sum[...] = (wide(proj, block_of(2), share) + wide(proj_in, share, share)).astype(bf16)
        mix_chip.start()

    def mix_finish():
        mix_chip.wait_recv()
        summed = (
            wide(proj, block_of(0), share)
            + wide(proj_in, 0, share)
            + proj_xin[...].astype(f32)
        )
        mixer_out_ref[...] = rms_scale(summed, mixer_gain_ref[...]).astype(bf16)

    def finish():
        for copy in give_back[1:]:
            copy.wait_recv()
        rest = slot_weight[...]
        combined = jnp.zeros((tok_rows, width), f32)
        for _ in range(3):
            piece = rest.astype(bf16)
            rest = rest - piece.astype(f32)
            combined = combined + lax.dot_general(
                piece, ret[...], (((0,), (0,)), ((), ())), preferred_element_type=f32
            )
        expert_out_ref[...] = rms_scale(combined, ffn_gain_ref[...]).astype(bf16)

    actions = {
        "F": forward,
        "D": lambda j: dispatch[j].start(),
        "R": pass_on,
        "P": reduce_core,
        "G": reduce_chip,
        "K": kv_stage,
        "A": attend,
    }
    single = {
        "KR": turn_keys,
        "W": lambda: None,
        "O": project,
        "M": mix_reduce,
        "N": mix_finish,
        "E": finish,
    }
    with jax.named_scope("route"):
        route()
    with jax.named_scope("barrier"):
        pl.semaphore_wait(barrier, len(peers))
    for step in STEPS:
        with jax.named_scope(step):
            if step in single:
                single[step]()
            elif step[0] == "C":
                compute([int(c) for c in step[1:]])
            else:
                actions[step[0]](int(step[1:]))
    with jax.named_scope("drain"):
        for copy in (
            [c for stage in kv_stages for c in stage]
            + dispatch[1:]
            + to_core
            + to_chip
            + relay
            + p_core
            + p_chip
            + give_back[1:]
            + mix_core
            + [mix_chip]
        ):
            copy.wait_send()


def fused_local(
    queries,
    keys,
    values,
    query_gain,
    key_gain,
    out_weight,
    mixer_gain,
    expert_in,
    routes,
    route_weights,
    expert_gain,
    gate_w,
    up_w,
    down_w,
    ffn_out_gain,
):
    n = lax.axis_size("ep")
    local_rows, query_width = queries.shape
    tok_rows, width = expert_in.shape
    cap = capacity_of(tok_rows, routes.shape[1], n)
    hidden = gate_w.shape[2]
    share = local_rows // 4
    vmem = pl.BlockSpec(memory_space=pltpu.VMEM)
    anywhere = pl.BlockSpec(memory_space=pl.ANY)
    bf16, f32 = jnp.bfloat16, jnp.float32
    dma = pltpu.SemaphoreType.DMA

    return pl.pallas_call(
        fused_kernel,
        out_shape=(
            jax.ShapeDtypeStruct((share, width), bf16),
            jax.ShapeDtypeStruct((tok_rows, width), bf16),
        ),
        in_specs=[anywhere] * 8 + [vmem] * 11,
        out_specs=(vmem, vmem),
        scratch_shapes=[
            pltpu.VMEM((local_rows, query_width), bf16),
            pltpu.VMEM((local_rows, HEAD), bf16),
            pltpu.VMEM((tok_rows, width), bf16),
            pltpu.VMEM((query_width, width), bf16),
            pltpu.VMEM((width, hidden), bf16),
            pltpu.VMEM((width, hidden), bf16),
            pltpu.VMEM((hidden, width), bf16),
            pltpu.VMEM((n * local_rows, 2 * HEAD), bf16),
            pltpu.VMEM((local_rows, query_width), bf16),
            pltpu.VMEM((local_rows, width), bf16),
            pltpu.VMEM((2 * share, width), bf16),
            pltpu.VMEM((share, width), bf16),
            pltpu.VMEM((share, width), bf16),
            pltpu.VMEM((n * cap, width), bf16),
            pltpu.VMEM((n * cap, tok_rows), f32),
            pltpu.VMEM((4 * n * cap, width), bf16),
            pltpu.VMEM((4 * n * cap, width), bf16),
            pltpu.VMEM((2 * n * cap, width), bf16),
            pltpu.VMEM((n * cap, width), bf16),
            pltpu.VMEM((n * cap, width), bf16),
            pltpu.VMEM((n * cap, width), bf16),
            pltpu.VMEM((n * cap, width), bf16),
            dma((8,)),
        ]
        + [dma((n,))] * 16
        + [dma((3,))] * 2,
        compiler_params=pltpu.CompilerParams(
            collective_id=0, has_side_effects=True, vmem_limit_bytes=60 * 2**20
        ),
    )(
        queries,
        keys,
        values,
        expert_in,
        out_weight,
        gate_w[0],
        up_w[0],
        down_w[0],
        query_gain[None],
        key_gain[None],
        mixer_gain[None],
        expert_gain[None],
        ffn_out_gain[None],
        routes.T,
        route_weights.T,
        *rope_tables(n * local_rows // GRID_W),
    )


def local(
    queries,
    keys,
    values,
    query_gain,
    key_gain,
    out_weight,
    mixer_gain,
    expert_in,
    routes,
    route_weights,
    expert_gain,
    gate_w,
    up_w,
    down_w,
    ffn_out_gain,
):
    if fused_fits(queries, keys, expert_in, routes, gate_w):
        return fused_local(
            queries, keys, values, query_gain, key_gain, out_weight, mixer_gain, expert_in, routes,
            route_weights, expert_gain, gate_w, up_w, down_w, ffn_out_gain,
        )
    mixer_out = mixer_half(queries, keys, values, query_gain, key_gain, out_weight, mixer_gain)
    expert_out = expert_half(
        expert_in, routes, route_weights, expert_gain, gate_w, up_w, down_w, ffn_out_gain
    )
    return (mixer_out, expert_out)


def solution(mesh):
    in_specs = (
        P("ep", "tp"),
        P("ep", "tp"),
        P("ep", "tp"),
        P(),
        P(),
        P("tp", None),
        P(),
        P(("ep", "tp"), None),
        P(("ep", "tp"), None),
        P(("ep", "tp"), None),
        P(),
        P("ep", None, "tp"),
        P("ep", None, "tp"),
        P("ep", "tp", None),
        P(),
    )
    out_specs = (P(("ep", "tp"), None), P(("ep", "tp"), None))
    return jax.shard_map(local, mesh=mesh, in_specs=in_specs, out_specs=out_specs, check_vma=False)
```

time: 123 us -> 91.3 us (0.74)
  Pallas kernels: 107 us -> 86.7 us
  other arithmetic: 7.51 us -> 0 us
  local copies, waits for them, and re-layouts: 5.87 us -> 3.5 us
  matrix products: 1.96 us -> 0 us
    pallas_call x1, Pallas kernels: 107 us -> 86.7 us  [fused_local(): pl.pallas_call(fused_kernel, out_shape=(jax.ShapeDtypeStruct((share, widt...]
    reduce_sum x3 -> x0, other arithmetic: 2.06 us -> none  [the longest x2 1.3 us: rms_scale(): jnp.mean(values_in * values_in, axis=-1, keepdims=True) + norm_eps]
    dot_general x2 -> x0, matrix products: 1.96 us -> none  [the longest x1 1.82 us: fused_local(): lax.dot_general(pick, normed, (((0,), (0,)), ((), ())), preferred_element...]
    concatenate x3 -> x0, other arithmetic: 1.65 us -> none  [the longest x1 0.66 us: fused_local(): jnp.concatenate([jnp.broadcast_to(query_gain, (heads, HEAD)), key_gain[No...]
    unnamed x12 -> x2, local copies, waits for them, and re-layouts: 3.52 us -> 3.5 us
where the time goes in v1:
time: 91.3 us; the launch traced here: 90.8 us
  Pallas kernels  86.7 us (95%)
  local copies, waits for them, and re-layouts  3.5 us (4%)
    pallas_call x1, Pallas kernels, fused_local(): pl.pallas_call(fused_kernel, out_shape=(jax.ShapeDtypeStruct((share, widt...  86.7 us
    unnamed x2, local copies, waits for them, and re-layouts  3.5 us

profile of v1, /device:TPU:9, one launch (start us, length us, event | category | flops | bytes accessed | tf_op | source)
XLA Modules:
  0.0 90.8 jit_solution(16019340128321257781)
XLA Ops:
  0.6 86.7 %shard_map.194 = (bf16[48,2048]{1,0:T(8,128)(2,1)}, bf16[128,2048]{1,0:T(8,128)(2,1)}) custom-call(bf16[192,512]{1,0:T(8,128)(2,1)} %query_hbm.1, bf16[192,128]{1,0:T(8,128)(2,1)} %key_hbm.1, bf16[192,128]{1,0:T(8,128)(2,1)} %value_hbm.1, bf16[128,2048]{1,0:T(8,128)(2,1)} %expert_hbm.1, bf16[512,2048]{1,0:T(8,128)(2,1)} %out_w_hbm.1, ...), custom_call_target="tpu_custom_call" | custom-call | tf_op jit(solution)/shard_map/pallas_call | solution.py:678
  87.3 1.6 %copy.23 = bf16[48,2048]{1,0:T(8,128)(2,1)} copy(bf16[48,2048]{1,0:T(8,128)(2,1)} %get-tuple-element.4) | data formatting | bytes 393216
  88.9 1.9 %copy.24 = bf16[128,2048]{1,0:T(8,128)(2,1)} copy(bf16[128,2048]{1,0:T(8,128)(2,1)} %get-tuple-element.5) | data formatting | bytes 1048576

commit v2 on v1

--- a/solution.py
+++ b/solution.py
@@ -203,14 +203,14 @@
 
 
 STEPS = (
-    "F0", "D2", "W", "D1", "KR", "D3", "K0", "F1", "D4", "F2", "F3", "R2", "R1", "R0", "D6",
-    "C2", "F4", "P2", "R3", "K1", "D5", "R4", "F6", "C4", "P4", "C1", "D7", "R6", "G2", "C3",
-    "P1", "G4", "K2", "F5", "C6", "P6", "G1", "F7", "R5", "C5", "G6", "P5", "P3", "R7", "C7",
-    "G5", "C0", "P7", "A0", "A1", "A2", "G3", "P0", "A3", "O", "M", "G7", "G0", "N", "E",
+    "D4", "D2", "D1", "KR", "F0", "F1", "D3", "R0", "K0", "D5", "F2", "F4", "K1", "F3", "F5",
+    "D7", "R1", "R4", "C4", "K2", "R2", "R3", "P4", "C3", "P3", "F7", "D6", "R5", "C5", "C1",
+    "P5", "G3", "C2", "A2", "G4", "R7", "F6", "G5", "A0", "P2", "A1", "C7", "R6", "C0", "P7",
+    "A3", "C6", "P1", "P6", "O", "G7", "P0", "M", "G1", "G2", "G6", "G0", "Q", "N", "E",
 )
 
 
-def rope_tables(grid_rows):
+def turn_table(grid_rows):
     half = HEAD // 2
     lane = np.arange(HEAD)
     inverse = rope_base ** (-2.0 * (lane % (half // 2)) / half)
@@ -219,12 +219,12 @@
     col = np.arange(GRID_W)[:, None] * inverse[None, :]
     low = (lane < half)[None, :]
     tables = (
+        np.where(low, 0.0, np.cos(col)),
+        np.where(low, 0.0, np.sin(col) * sign),
         np.where(low, np.cos(row), 0.0),
         np.where(low, np.sin(row) * sign, 0.0),
-        np.where(low, 0.0, np.cos(col)),
-        np.where(low, 0.0, np.sin(col) * sign),
-    )
-    return [jnp.asarray(t.astype(np.float32)) for t in tables]
+    )
+    return jnp.asarray(np.concatenate(tables).astype(np.float32))
 
 
 def fused_kernel(
@@ -236,19 +236,24 @@
     gate_hbm,
     up_hbm,
     down_hbm,
+    expert_gain_hbm,
+    routes_hbm,
+    route_weight_hbm,
+    query_gain_hbm,
+    key_gain_hbm,
+    turn_hbm,
+    mixer_gain_hbm,
+    ffn_gain_hbm,
+    mixer_out_ref,
+    expert_out_ref,
+    expert_gain_ref,
+    routes_ref,
+    route_weight_ref,
     query_gain_ref,
     key_gain_ref,
+    turn_ref,
     mixer_gain_ref,
-    expert_gain_ref,
     ffn_gain_ref,
-    routes_ref,
-    route_weight_ref,
-    row_cos_ref,
-    row_sin_ref,
-    col_cos_ref,
-    col_sin_ref,
-    mixer_out_ref,
-    expert_out_ref,
     query,
     key,
     expert_in,
@@ -271,6 +276,7 @@
     part_xin,
     final,
     ret,
+    combined,
     load_sem,
     kv_send,
     kv_recv,
@@ -314,28 +320,6 @@
             device_id_type=pl.DeviceIdType.MESH,
         )
 
-    loads = {
-        name: pltpu.make_async_copy(a, b, load_sem.at[i])
-        for i, (name, a, b) in enumerate(
-            [
-                ("expert", expert_hbm, expert_in),
-                ("key", key_hbm, key),
-                ("value", value_hbm, kv_all.at[pl.ds(0, local_rows), pl.ds(HEAD, HEAD)]),
-                ("query", query_hbm, query),
-                ("gate", gate_hbm, gate),
-                ("up", up_hbm, up),
-                ("down", down_hbm, down),
-                ("out", out_w_hbm, out_w),
-            ]
-        )
-    }
-    for load in loads.values():
-        load.start()
-
-    def settle(name):
-        if name in loads:
-            loads.pop(name).wait()
-
     barrier = pltpu.get_barrier_semaphore()
     peers = [(j, 0) for j in range(1, n)] + [(0, 1), (0, 2)]
     for ep_bits, tp_bits in peers:
@@ -345,6 +329,38 @@
             device_id={"ep": flip(ep, ep_bits), "tp": flip(tp, tp_bits)},
             device_id_type=pl.DeviceIdType.MESH,
         )
+
+    loads = {
+        name: pltpu.make_async_copy(a, b, load_sem.at[i])
+        for i, (name, a, b) in enumerate(
+            [
+                ("expert", expert_hbm, expert_in),
+                ("routes", routes_hbm, routes_ref),
+                ("route_weight", route_weight_hbm, route_weight_ref),
+                ("expert_gain", expert_gain_hbm, expert_gain_ref),
+                ("query_gain", query_gain_hbm, query_gain_ref),
+                ("key_gain", key_gain_hbm, key_gain_ref),
+                ("turn", turn_hbm, turn_ref),
+                ("key", key_hbm, key),
+                ("value", value_hbm, kv_all.at[pl.ds(0, local_rows), pl.ds(HEAD, HEAD)]),
+                ("query", query_hbm, query),
+                ("gate", gate_hbm, gate),
+                ("up", up_hbm, up),
+                ("down", down_hbm, down),
+                ("out", out_w_hbm, out_w),
+                ("mixer_gain", mixer_gain_hbm, mixer_gain_ref),
+                ("ffn_gain", ffn_gain_hbm, ffn_gain_ref),
+            ]
+        )
+    }
+
+    for load in loads.values():
+        load.start()
+
+    def settle(*names):
+        for name in names:
+            if name in loads:
+                loads.pop(name).wait()
 
     kv_stages = []
     held = [0]
@@ -430,8 +446,7 @@
         )
 
     def route():
-        settle("expert")
-        normed = rms_scale(expert_in[...].astype(f32), expert_gain_ref[...]).astype(bf16)
+        settle("routes", "route_weight")
         number = lax.broadcasted_iota(jnp.int32, (n, tok_rows), 0)
         number = jnp.bitwise_xor(number, ep.astype(jnp.int32))
         chosen = jnp.zeros((n, tok_rows), f32)
@@ -453,6 +468,8 @@
             picks.append(jnp.where(taken, 1.0, 0.0))
             slot_weight[j * cap : (j + 1) * cap, :] = jnp.where(taken, weight[j : j + 1, :], 0.0)
         pick = jnp.concatenate(picks, axis=0).astype(bf16)
+        settle("expert", "expert_gain")
+        normed = rms_scale(expert_in[...].astype(f32), expert_gain_ref[...]).astype(bf16)
         out = jnp.dot(pick, normed, preferred_element_type=f32).astype(bf16)
         rows[0:cap, :] = out[0:cap, :]
         outg[cap:, :] = out[cap:, :]
@@ -467,16 +484,17 @@
             pltpu.roll(field, HEAD // 4, axis=1),
         )
         pieces = []
+        all_rows = n * grid_rows
         for r in range(grid_rows):
             span = slice(r * GRID_W, (r + 1) * GRID_W)
-            line = pl.ds(ep * grid_rows + r, 1)
-            cosine = row_cos_ref[line, :] + col_cos_ref[...]
-            sine = row_sin_ref[line, :] + col_sin_ref[...]
+            line = 2 * GRID_W + ep * grid_rows + r
+            cosine = turn_ref[pl.ds(line, 1), :] + turn_ref[0:GRID_W, :]
+            sine = turn_ref[pl.ds(line + all_rows, 1), :] + turn_ref[GRID_W : 2 * GRID_W, :]
             pieces.append(field[span] * cosine + partner[span] * sine)
         return jnp.concatenate(pieces, axis=0).astype(bf16)
 
     def turn_keys():
-        settle("key")
+        settle("key", "key_gain", "turn")
         kv_all[0:local_rows, 0:HEAD] = turned(key[...], key_gain_ref[...])
         settle("value")
 
@@ -537,7 +555,7 @@
             copy.start()
 
     def attend(head):
-        settle("query")
+        settle("query", "query_gain", "turn")
         while kv_last:
             kv_last.pop().wait_recv()
         column = slice(head * HEAD, (head + 1) * HEAD)
@@ -582,6 +600,7 @@
 
     def mix_finish():
         mix_chip.wait_recv()
+        settle("mixer_gain")
         summed = (
             wide(proj, block_of(0), share)
             + wide(proj_in, 0, share)
@@ -589,18 +608,30 @@
         )
         mixer_out_ref[...] = rms_scale(summed, mixer_gain_ref[...]).astype(bf16)
 
-    def finish():
-        for copy in give_back[1:]:
-            copy.wait_recv()
-        rest = slot_weight[...]
-        combined = jnp.zeros((tok_rows, width), f32)
+    def weighted(start, size):
+        rest = slot_weight[start : start + size, :]
+        total = None
         for _ in range(3):
             piece = rest.astype(bf16)
             rest = rest - piece.astype(f32)
-            combined = combined + lax.dot_general(
-                piece, ret[...], (((0,), (0,)), ((), ())), preferred_element_type=f32
+            term = lax.dot_general(
+                piece,
+                ret[start : start + size, :],
+                (((0,), (0,)), ((), ())),
+                preferred_element_type=f32,
             )
-        expert_out_ref[...] = rms_scale(combined, ffn_gain_ref[...]).astype(bf16)
+            total = term if total is None else total + term
+        return total
+
+    def gather():
+        for copy in give_back[1:]:
+            copy.wait_recv()
+        combined[...] = weighted(cap, (n - 1) * cap)
+
+    def finish():
+        settle("ffn_gain")
+        total = combined[...] + weighted(0, cap)
+        expert_out_ref[...] = rms_scale(total, ffn_gain_ref[...]).astype(bf16)
 
     actions = {
         "F": forward,
@@ -613,10 +644,10 @@
     }
     single = {
         "KR": turn_keys,
-        "W": lambda: None,
         "O": project,
         "M": mix_reduce,
         "N": mix_finish,
+        "Q": gather,
         "E": finish,
     }
     with jax.named_scope("route"):
@@ -670,6 +701,7 @@
     cap = capacity_of(tok_rows, routes.shape[1], n)
     hidden = gate_w.shape[2]
     share = local_rows // 4
+    table = turn_table(n * local_rows // GRID_W)
     vmem = pl.BlockSpec(memory_space=pltpu.VMEM)
     anywhere = pl.BlockSpec(memory_space=pl.ANY)
     bf16, f32 = jnp.bfloat16, jnp.float32
@@ -678,12 +710,20 @@
     return pl.pallas_call(
         fused_kernel,
         out_shape=(
-            jax.ShapeDtypeStruct((share, width), bf16),
-            jax.ShapeDtypeStruct((tok_rows, width), bf16),
+            pltpu.VMEM((share, width), bf16),
+            pltpu.VMEM((tok_rows, width), bf16),
         ),
-        in_specs=[anywhere] * 8 + [vmem] * 11,
+        in_specs=[anywhere] * 16,
         out_specs=(vmem, vmem),
         scratch_shapes=[
+            pltpu.VMEM((1, width), f32),
+            pltpu.VMEM((routes.shape[1], tok_rows), jnp.int32),
+            pltpu.VMEM((routes.shape[1], tok_rows), f32),
+            pltpu.VMEM((1, HEAD), f32),
+            pltpu.VMEM((1, HEAD), f32),
+            pltpu.VMEM(table.shape, f32),
+            pltpu.VMEM((1, width), f32),
+            pltpu.VMEM((1, width), f32),
             pltpu.VMEM((local_rows, query_width), bf16),
             pltpu.VMEM((local_rows, HEAD), bf16),
             pltpu.VMEM((tok_rows, width), bf16),
@@ -706,7 +746,8 @@
             pltpu.VMEM((n * cap, width), bf16),
             pltpu.VMEM((n * cap, width), bf16),
             pltpu.VMEM((n * cap, width), bf16),
-            dma((8,)),
+            pltpu.VMEM((tok_rows, width), f32),
+            dma((16,)),
         ]
         + [dma((n,))] * 16
         + [dma((3,))] * 2,
@@ -722,14 +763,14 @@
         gate_w[0],
         up_w[0],
         down_w[0],
+        expert_gain[None],
+        routes.T,
+        route_weights.T,
         query_gain[None],
         key_gain[None],
+        table,
         mixer_gain[None],
-        expert_gain[None],
         ffn_out_gain[None],
-        routes.T,
-        route_weights.T,
-        *rope_tables(n * local_rows // GRID_W),
     )
 
 

time: 91.3 us -> 86.9 us (0.952)
  Pallas kernels: 86.7 us -> 83.9 us
  local copies, waits for them, and re-layouts: 3.5 us -> 1.47 us
    pallas_call x1, Pallas kernels: 86.7 us -> 83.9 us  [fused_local(): pl.pallas_call(fused_kernel, out_shape=(pltpu.VMEM((share, width), bf16),...]
    unnamed x2, local copies, waits for them, and re-layouts: 3.5 us -> 1.47 us
where the time goes in v2:
time: 86.9 us; the launch traced here: 86 us
  Pallas kernels  83.9 us (97%)
  local copies, waits for them, and re-layouts  1.47 us (2%)
    pallas_call x1, Pallas kernels, fused_local(): pl.pallas_call(fused_kernel, out_shape=(pltpu.VMEM((share, width), bf16),...  83.9 us

profile of v2, /device:TPU:9, one launch (start us, length us, event | category | flops | bytes accessed | tf_op | source)
XLA Modules:
  0.0 86.0 jit_solution(3095545441125321617)
XLA Ops:
  0.6 83.9 %shard_map.167 = (bf16[48,2048]{1,0:T(8,128)(2,1)S(1)}, bf16[128,2048]{1,0:T(8,128)(2,1)S(1)}) custom-call(bf16[192,512]{1,0:T(8,128)(2,1)} %query_hbm.1, bf16[192,128]{1,0:T(8,128)(2,1)} %key_hbm.1, bf16[192,128]{1,0:T(8,128)(2,1)} %value_hbm.1, bf16[128,2048]{1,0:T(8,128)(2,1)} %expert_hbm.1, bf16[512,2048]{1,0:T(8,128)(2,1)} %out_w_hbm.1, ...), custom_call_target="tpu_custom_call" | custom-call | tf_op jit(solution)/shard_map/pallas_call | solution.py:710
  84.5 0.7 copy.20
  85.2 0.8 copy.21

commit v3 on v2

--- a/solution.py
+++ b/solution.py
@@ -203,7 +203,7 @@
 
 
 STEPS = (
-    "D4", "D2", "D1", "KR", "F0", "F1", "D3", "R0", "K0", "D5", "F2", "F4", "K1", "F3", "F5",
+    "D4", "D2", "D1", "KR", "F0", "F1", "D3", "R0", "K0", "D5", "F4", "F2", "K1", "F3", "F5",
     "D7", "R1", "R4", "C4", "K2", "R2", "R3", "P4", "C3", "P3", "F7", "D6", "R5", "C5", "C1",
     "P5", "G3", "C2", "A2", "G4", "R7", "F6", "G5", "A0", "P2", "A1", "C7", "R6", "C0", "P7",
     "A3", "C6", "P1", "P6", "O", "G7", "P0", "M", "G1", "G2", "G6", "G0", "Q", "N", "E",
@@ -321,7 +321,7 @@
         )
 
     barrier = pltpu.get_barrier_semaphore()
-    peers = [(j, 0) for j in range(1, n)] + [(0, 1), (0, 2)]
+    peers = [(1 << b, 0) for b in range(n.bit_length() - 1)] + [(0, 1), (0, 2)]
     for ep_bits, tp_bits in peers:
         pl.semaphore_signal(
             barrier,

time: 86.9 us -> 86.2 us (level)
  no operation moved by 1% of the time
where the time goes in v3:
time: 86.2 us; the launch traced here: 86 us
  Pallas kernels  83.9 us (97%)
  local copies, waits for them, and re-layouts  1.47 us (2%)
    pallas_call x1, Pallas kernels, fused_local(): pl.pallas_call(fused_kernel, out_shape=(pltpu.VMEM((share, width), bf16),...  83.9 us

profile of v3, /device:TPU:9, one launch (start us, length us, event | category | flops | bytes accessed | tf_op | source)
XLA Modules:
  0.0 86.0 jit_solution(15248779601260091)
XLA Ops:
  0.6 83.9 %shard_map.167 = (bf16[48,2048]{1,0:T(8,128)(2,1)S(1)}, bf16[128,2048]{1,0:T(8,128)(2,1)S(1)}) custom-call(bf16[192,512]{1,0:T(8,128)(2,1)} %query_hbm.1, bf16[192,128]{1,0:T(8,128)(2,1)} %key_hbm.1, bf16[192,128]{1,0:T(8,128)(2,1)} %value_hbm.1, bf16[128,2048]{1,0:T(8,128)(2,1)} %expert_hbm.1, bf16[512,2048]{1,0:T(8,128)(2,1)} %out_w_hbm.1, ...), custom_call_target="tpu_custom_call" | custom-call | tf_op jit(solution)/shard_map/pallas_call | solution.py:710
  84.5 0.7 copy.20
  85.2 0.8 copy.21
